TPU v7x, 32 devices: a whole 2x2x4 slice. The times are simulated.
32 devices in a mesh: sp: 4 (over y, x), tp: 8 (over z, core).
Axes of the slice: x: 2, y: 2, z: 4, core: 2. Of those that a mesh axis runs over, the one named last changes fastest.
Arguments:
- tokens: bfloat16 [2048, 4096], P('sp', 'tp'), may hold values from -6 to 6
- pre_gain: float32 [2, 4096], replicated, may hold values from 0.1 to 1.9
- w_value: bfloat16 [2, 4096, 4096], P(None, 'sp', 'tp'), may hold values from -0.09375 to 0.09375
- w_gate: bfloat16 [2, 4096, 4096], P(None, 'sp', 'tp'), may hold values from -0.09375 to 0.09375
- conv_taps: float32 [2, 31, 4096], P(None, None, 'tp'), may hold values from -3.5 to 3.5
- conv_bias: float32 [2, 4096], P(None, 'tp'), may hold values from -3 to 3
- norm_gain: float32 [2, 4096], P(None, 'tp'), may hold values from 0.1 to 1.9
- norm_bias: float32 [2, 4096], P(None, 'tp'), may hold values from -3 to 3
- w_out: bfloat16 [2, 4096, 4096], P(None, 'sp', 'tp'), may hold values from -0.09375 to 0.09375
- post_gain: float32 [2, 4096], P(None, 'tp'), may hold values from 0.1 to 1.9
Outputs:
- stream: bfloat16 [2048, 4096], P('sp', 'tp')
All inputs are finite; a program needn't handle non-finite values.
Results may differ from a plain program's by a relative error of at most 0.009.
Values may be sent and summed in bfloat16 or wider, within the bound.
A program may use at most 64 MiB of HBM per device.

v0:
```python
import jax
import jax.numpy as jnp
from jax import lax
from jax.sharding import PartitionSpec as P


def passed_along(value, axis, steps):
    count = lax.axis_size(axis)
    leading, last = (max(0, -steps), min(count, count - steps))
    return lax.ppermute(value, axis, [(source, source + steps) for source in range(leading, last)])


def shards(
    tokens, pre_gain, w_value, w_gate, conv_taps, conv_bias, norm_gain, norm_bias, w_out, post_gain
):
    layer_count = w_value.shape[0]
    tap_count = conv_taps.shape[1]
    channel_count = conv_taps.shape[2] * lax.axis_size("tp")
    model_width = tokens.shape[1] * lax.axis_size("tp")
    local_rows = tokens.shape[0]
    every_value, every_gate, every_out = (
        lax.all_gather(w_value, "sp", axis=1, tiled=True),
        lax.all_gather(w_gate, "sp", axis=1, tiled=True),
        lax.all_gather(w_out, "sp", axis=1, tiled=True),
    )
    stream = tokens
    for layer_index in range(layer_count):
        gathered = lax.all_gather(stream, "tp", axis=1, tiled=True)
        full_rows = gathered.astype(jnp.float32)
        scale_rows = lax.rsqrt(jnp.mean(full_rows * full_rows, axis=-1, keepdims=True) + 1e-06)
        normed = (full_rows * scale_rows * pre_gain[layer_index]).astype(jnp.bfloat16)
        value_block = every_value[layer_index]
        gate_block = every_gate[layer_index]
        out_block = every_out[layer_index]
        value_proj = jnp.dot(normed, value_block, preferred_element_type=jnp.float32)
        gate_proj = jnp.dot(normed, gate_block, preferred_element_type=jnp.float32)
        glu_out = (value_proj * jax.nn.sigmoid(gate_proj)).astype(jnp.bfloat16)
        earlier = passed_along(glu_out[local_rows - (tap_count - 1) :], "sp", 1)
        padded = jnp.concatenate([earlier, glu_out], axis=0).astype(jnp.float32)
        filtered = jnp.zeros(glu_out.shape, jnp.float32) + conv_bias[layer_index]
        for tap_index in range(tap_count):
            filtered = (
                filtered
                + padded[tap_index : tap_index + local_rows] * conv_taps[layer_index, tap_index]
            )
        channel_sum, channel_square = lax.psum(
            (jnp.sum(filtered, axis=-1), jnp.sum(filtered * filtered, axis=-1)), "tp"
        )
        centre = channel_sum / channel_count
        spread = jnp.maximum(channel_square / channel_count - centre * centre, 0.0)
        shaped = (filtered - centre[:, None]) * lax.rsqrt(spread + 1e-05)[:, None]
        mixed = jax.nn.silu(shaped * norm_gain[layer_index] + norm_bias[layer_index]).astype(
            jnp.bfloat16
        )
        whole_mixed = lax.all_gather(mixed, "tp", axis=1, tiled=True)
        branch_low = jnp.dot(whole_mixed, out_block, preferred_element_type=jnp.float32).astype(
            jnp.bfloat16
        )
        branch = lax.optimization_barrier(branch_low).astype(jnp.float32)
        total = lax.psum(jnp.sum(branch * branch, axis=-1), "tp")
        rescale = lax.rsqrt(total / model_width + 1e-06)[:, None]
        stream = (stream.astype(jnp.float32) + branch * rescale * post_gain[layer_index]).astype(
            jnp.bfloat16
        )
    return stream


def solution(mesh):
    in_specs = (
        P("sp", "tp"),
        P(),
        P(None, "sp", "tp"),
        P(None, "sp", "tp"),
        P(None, None, "tp"),
        P(None, "tp"),
        P(None, "tp"),
        P(None, "tp"),
        P(None, "sp", "tp"),
        P(None, "tp"),
    )
    out_specs = P("sp", "tp")
    return jax.shard_map(shards, mesh=mesh, in_specs=in_specs, out_specs=out_specs, check_vma=False)
```

profile of v0, /device:TPU:0, one launch (start us, length us, event | category | flops | bytes accessed | tf_op | source)
XLA Modules:
  0.0 551.2 jit_solution(2232420375245703278)
XLA Ops:
  6.5 0.0 all-gather.8.cloned.1.call-start
  6.6 0.7 all-gather.8.cloned.1.call-update
  7.3 0.0 all-gather.12.cloned.1.call-start
  7.3 0.7 all-gather.12.cloned.1.call-update
  8.0 0.0 all-gather.10.cloned.1.call-start
  8.1 0.7 all-gather.10.cloned.1.call-update
  8.8 0.0 all-gather.16.cloned.1.call-start
  8.8 0.5 all-gather.16.cloned.1.call-update
  9.3 0.0 all-gather.14.cloned.1.call-start
  9.6 49.0 %all-gather.8.cloned.1.call-done = bf16[512,4096]{1,0:T(8,128)(2,1)} async-done(((bf16[512,512]{1,0:T(8,128)(2,1)}), bf16[512,4096]{1,0:T(8,128)(2,1)}) %all-gather.8.cloned.1.call-update) | async-done | bytes 4194320 | tf_op jit(solution)/shard_map/all_gather | solution.py:28
  58.6 3.1 fusion
  61.7 85.1 %all-gather.12.cloned.1.call-done = bf16[2,4096,512]{2,1,0:T(8,128)(2,1)} async-done(((bf16[2,1024,512]{2,1,0:T(8,128)(2,1)}), bf16[2,4096,512]{2,1,0:T(8,128)(2,1)}) %all-gather.12.cloned.1.call-update) | async-done | bytes 8388624 | tf_op jit(solution)/shard_map/all_gather | solution.py:23
  146.7 6.0 %fusion.21 = f32[512,512]{1,0:T(8,128)S(1)} fusion(bf16[2,4096,512]{2,1,0:T(8,128)(2,1)} %all-gather.12.cloned.1.call-done, bf16[512,4096]{1,0:T(8,128)(2,1)} %all-gather.8.cloned.1.call-done, f32[4096]{0:T(1024)S(1)} %bitcast.122, f32[512]{0:T(512)S(1)} %add_rsqrt_fusion.5), kind=kOutput, calls=%fused_computation.35 | convolution fusion | flops 2156658688 | bytes 9455616 | tf_op jit(solution)/shard_map/dot_general | solution.py:36
  152.7 83.4 %all-gather.10.cloned.1.call-done = bf16[2,4096,512]{2,1,0:T(8,128)(2,1)} async-done(((bf16[2,1024,512]{2,1,0:T(8,128)(2,1)}), bf16[2,4096,512]{2,1,0:T(8,128)(2,1)}) %all-gather.10.cloned.1.call-update) | async-done | bytes 8388624 | tf_op jit(solution)/shard_map/all_gather | solution.py:22
  236.1 5.8 %fusion.23 = bf16[512,512]{1,0:T(8,128)(2,1)S(1)} fusion(f32[512,512]{1,0:T(8,128)S(1)} %fusion.21, bf16[2,4096,512]{2,1,0:T(8,128)(2,1)} %all-gather.10.cloned.1.call-done, bf16[512,4096]{1,0:T(8,128)(2,1)} %all-gather.8.cloned.1.call-done, f32[4096]{0:T(1024)S(1)} %bitcast.123, f32[512]{0:T(512)S(1)} %add_rsqrt_fusion.5), kind=kOutput, calls=%fused_computation.37 | convolution fusion | flops 2156396544 | bytes 9979904 | tf_op jit(solution)/shard_map/dot_general | solution.py:35
  242.0 3.4 collective-permute-start
  245.4 1.6 collective-permute-done
  246.9 0.2 maximum_convert_fusion
  247.1 5.0 fusion.101
  252.1 15.3 %all-reduce.1 = (f32[512]{0:T(512)S(1)}, f32[512]{0:T(512)S(1)}) all-reduce(f32[512]{0:T(512)S(1)} %get-tuple-element.8, f32[512]{0:T(512)S(1)} %get-tuple-element.7), channel_id=1, replica_groups=mesh['sp'=4,'tp'=8] {'tp'}, use_global_device_ids=true, to_apply=%region_4.0 | all-reduce | flops 1024 | bytes 8192 | tf_op jit(solution)/shard_map/psum | solution.py:46
  267.4 1.2 multiply_convert_fusion.1
  268.7 0.0 all-gather.14.cloned.1.call-update
  268.7 0.0 all-gather.18.cloned.1.call-start
  268.8 56.5 %all-gather.16.cloned.1.call-done = bf16[2,4096,512]{2,1,0:T(8,128)(2,1)} async-done(((bf16[2,1024,512]{2,1,0:T(8,128)(2,1)}), bf16[2,4096,512]{2,1,0:T(8,128)(2,1)}) %all-gather.16.cloned.1.call-update) | async-done | bytes 8388624 | tf_op jit(solution)/shard_map/all_gather | solution.py:24
  325.3 48.4 %all-gather.14.cloned.1.call-done = bf16[512,4096]{1,0:T(8,128)(2,1)} async-done(((bf16[512,512]{1,0:T(8,128)(2,1)}), bf16[512,4096]{1,0:T(8,128)(2,1)}) %all-gather.14.cloned.1.call-update) | async-done | bytes 4194320 | tf_op jit(solution)/shard_map/all_gather | solution.py:55
  373.7 5.8 %fusion.24 = bf16[512,512]{1,0:T(8,128)(2,1)S(1)} fusion(bf16[512,4096]{1,0:T(8,128)(2,1)} %all-gather.14.cloned.1.call-done, bf16[2,4096,512]{2,1,0:T(8,128)(2,1)} %all-gather.16.cloned.1.call-done), kind=kOutput, calls=%fused_computation.38 | convolution fusion | flops 2147745792 | bytes 8912896 | tf_op jit(solution)/shard_map/dot_general | solution.py:56
  379.5 0.2 fusion.30
  379.6 14.8 %psum.44 = f32[512]{0:T(512)S(1)} all-reduce(f32[512]{0:T(512)S(1)} %fusion.30), channel_id=1, replica_groups=mesh['sp'=4,'tp'=8] {'tp'}, use_global_device_ids=true, to_apply=%region_6.7 | all-reduce | flops 512 | bytes 4096 | tf_op jit(solution)/shard_map/psum | solution.py:60
  394.5 1.1 fusion.33
  395.5 0.0 all-gather.18.cloned.1.call-update
  395.5 0.2 all-gather.20.cloned.1.call-start
  395.8 44.7 %all-gather.18.cloned.1.call-done = bf16[512,4096]{1,0:T(8,128)(2,1)} async-done(((bf16[512,512]{1,0:T(8,128)(2,1)}), bf16[512,4096]{1,0:T(8,128)(2,1)}) %all-gather.18.cloned.1.call-update) | async-done | bytes 4194320 | tf_op jit(solution)/shard_map/all_gather | solution.py:28
  440.5 3.2 fusion.3
  443.7 0.2 copy-done.1
  443.9 5.0 fusion.19
  449.0 2.4 fusion.22
  451.4 3.4 collective-permute-start.1
  454.9 1.5 collective-permute-done.1
  456.4 0.2 maximum_convert_fusion.1
  456.5 5.0 fusion.100
  461.6 13.7 %all-reduce = (f32[512]{0:T(512)S(1)}, f32[512]{0:T(512)S(1)}) all-reduce(f32[512]{0:T(512)S(1)} %get-tuple-element.6, f32[512]{0:T(512)S(1)} %get-tuple-element.5), channel_id=1, replica_groups=mesh['sp'=4,'tp'=8] {'tp'}, use_global_device_ids=true, to_apply=%region_11.12 | all-reduce | flops 1024 | bytes 8192 | tf_op jit(solution)/shard_map/psum | solution.py:46
  475.3 1.3 multiply_convert_fusion
  476.6 0.0 all-gather.20.cloned.1.call-update
  476.6 45.9 %all-gather.20.cloned.1.call-done = bf16[512,4096]{1,0:T(8,128)(2,1)} async-done(((bf16[512,512]{1,0:T(8,128)(2,1)}), bf16[512,4096]{1,0:T(8,128)(2,1)}) %all-gather.20.cloned.1.call-update) | async-done | bytes 4194320 | tf_op jit(solution)/shard_map/all_gather | solution.py:55
  522.5 5.8 %fusion.25 = bf16[512,512]{1,0:T(8,128)(2,1)S(1)} fusion(bf16[512,4096]{1,0:T(8,128)(2,1)} %all-gather.20.cloned.1.call-done, bf16[2,4096,512]{2,1,0:T(8,128)(2,1)} %all-gather.16.cloned.1.call-done), kind=kOutput, calls=%fused_computation.39 | convolution fusion | flops 2147745792 | bytes 8912896 | tf_op jit(solution)/shard_map/dot_general | solution.py:56
  528.3 0.2 fusion.34
  528.5 14.8 %psum.47 = f32[512]{0:T(512)S(1)} all-reduce(f32[512]{0:T(512)S(1)} %fusion.34), channel_id=1, replica_groups=mesh['sp'=4,'tp'=8] {'tp'}, use_global_device_ids=true, to_apply=%region_13.14 | all-reduce | flops 512 | bytes 4096 | tf_op jit(solution)/shard_map/psum | solution.py:60
  543.3 1.1 fusion.37
  (39 shorter events, 0.3 us)
Async XLA Ops:
  6.5 2.8 copy-start.5
  6.5 2.9 copy-start.6
  6.5 2.9 copy-start.3
  6.5 3.0 copy-start.4
  6.5 52.0 %all-gather.8.cloned.1.call-start = ((), (), s32[]{:S(2)}) async-start(), calls=%async_computation | async-start | bytes 4718592 | tf_op jit(solution)/shard_map/all_gather | solution.py:28
  7.3 139.5 %all-gather.12.cloned.1.call-start = ((), (), s32[]{:S(2)}) async-start(), calls=%async_computation.2 | async-start | bytes 10485760 | tf_op jit(solution)/shard_map/all_gather | solution.py:23
  8.0 228.1 %all-gather.10.cloned.1.call-start = ((), (), s32[]{:S(2)}) async-start(), calls=%async_computation.1 | async-start | bytes 10485760 | tf_op jit(solution)/shard_map/all_gather | solution.py:22
  8.8 316.6 %all-gather.16.cloned.1.call-start = ((), (), s32[]{:S(2)}) async-start(), calls=%async_computation.4 | async-start | bytes 10485760 | tf_op jit(solution)/shard_map/all_gather | solution.py:24
  9.3 364.3 %all-gather.14.cloned.1.call-start = ((), (), s32[]{:S(2)}) async-start(), calls=%async_computation.3 | async-start | bytes 4718592 | tf_op jit(solution)/shard_map/all_gather | solution.py:55
  152.7 92.6 %copy-start.7 = (f32[2,512]{1,0:T(2,128)S(1)}, f32[2,512]{1,0:T(2,128)}, u32[]{:S(2)}) copy-start(f32[2,512]{1,0:T(2,128)} %param.16) | copy-start | bytes 12292
  242.0 5.0 collective-permute-start
  247.1 21.7 %copy-start.8 = (f32[2,512]{1,0:T(2,128)S(1)}, f32[2,512]{1,0:T(2,128)}, u32[]{:S(2)}) copy-start(f32[2,512]{1,0:T(2,128)} %param.19) | copy-start | bytes 12292
  268.7 171.8 %all-gather.18.cloned.1.call-start = ((), (), s32[]{:S(2)}) async-start(), calls=%async_computation.5 | async-start | bytes 4718592 | tf_op jit(solution)/shard_map/all_gather | solution.py:28
  268.8 125.7 %copy-start.2 = (bf16[512,512]{1,0:T(8,128)(2,1)S(1)}, bf16[512,512]{1,0:T(8,128)(2,1)}, u32[]{:S(2)}) copy-start(bf16[512,512]{1,0:T(8,128)(2,1)} %param.10) | copy-start | bytes 1572868
  395.5 127.0 %all-gather.20.cloned.1.call-start = ((), (), s32[]{:S(2)}) async-start(), calls=%async_computation.6 | async-start | bytes 4718592 | tf_op jit(solution)/shard_map/all_gather | solution.py:55
  440.5 3.4 copy-start.1
  440.5 8.5 %slice-start = ((s8[8388608]{0:T(1024)(128)(4,1)}), s8[4194304]{0:T(1024)(128)(4,1)S(1)}, s32[]{:S(2)}) async-start(s8[8388608]{0:T(1024)(128)(4,1)} %bitcast.194), calls=%async_computation.7 | async-start | bytes 8388608
  443.9 5.0 slice-start.1
  451.4 5.0 collective-permute-start.1
  476.6 66.7 %copy-start = (bf16[512,512]{1,0:T(8,128)(2,1)S(1)}, bf16[512,512]{1,0:T(8,128)(2,1)}, u32[]{:S(2)}) copy-start(bf16[512,512]{1,0:T(8,128)(2,1)} %fusion.33) | copy-start | bytes 1572868
Sparse Core Ops, SparseCore 0:
  9.0 49.5 all-gather.7
  60.4 86.2 all-gather.11
  148.6 87.4 all-gather.9
  237.8 87.4 all-gather.15
  326.8 46.8 all-gather.13
  395.7 44.7 all-gather.17
  476.7 45.7 all-gather.19
where the time goes:
time: 551 us
  waiting for transfers between devices  419 us (76%)
  blocking collectives  58.7 us (11%)
  matrix products  30.8 us (6%)
  other arithmetic  21.7 us (4%)
  between operations  13.8 us (3%)
  starting transfers between devices  7.2 us (1%)
    all_gather x2, waiting for transfers between devices, shards(): whole_mixed = lax.all_gather(mixed, 'tp', axis=1, tiled=True)  94.2 us
    all_gather x2, waiting for transfers between devices, shards(): gathered = lax.all_gather(stream, 'tp', axis=1, tiled=True)  93.7 us
    all_gather x1, waiting for transfers between devices, shards(): lax.all_gather(w_gate, 'sp', axis=1, tiled=True)  85.1 us
    all_gather x1, waiting for transfers between devices, shards(): lax.all_gather(w_value, 'sp', axis=1, tiled=True)  83.4 us
    all_gather x1, waiting for transfers between devices, shards(): lax.all_gather(w_out, 'sp', axis=1, tiled=True)  56.5 us
    psum x2, blocking collectives, shards(): total = lax.psum(jnp.sum(branch * branch, axis=-1), 'tp')  29.6 us
    psum x2, blocking collectives, shards(): lax.psum((jnp.sum(filtered, axis=-1), jnp.sum(filtered * filtered, axis=-...  29.1 us
    dot_general x2, matrix products, shards(): jnp.dot(whole_mixed, out_block, preferred_element_type=jnp.float32)  11.6 us
  transfers between devices with their start and end apart: 9, of which 9 were waited for; matrix products, arithmetic and copies ran while one was open for 4% of the time, Pallas kernels for 0%

commit v1 on v0

--- a/solution.py
+++ b/solution.py
@@ -1,7 +1,190 @@
+import functools
+
 import jax
 import jax.numpy as jnp
 from jax import lax
+from jax.experimental import pallas as pl
+from jax.experimental.pallas import tpu as pltpu
 from jax.sharding import PartitionSpec as P
+
+MESH = pl.DeviceIdType.MESH
+
+
+def gather_kernel(chips, x_ref, out_ref, up_send, up_recv, down_send, down_recv, side_send, side_recv):
+    me = lax.axis_index("tp")
+    z = me // 2
+    core = me - 2 * z
+    partner = me + 1 - 2 * core
+    width = x_ref.shape[1]
+    has_up = z < chips - 1
+    has_down = z > 0
+
+    barrier = pltpu.get_barrier_semaphore()
+    pl.semaphore_signal(barrier, inc=1, device_id={"tp": partner}, device_id_type=MESH)
+
+    @pl.when(has_up)
+    def _():
+        pl.semaphore_signal(barrier, inc=1, device_id={"tp": me + 2}, device_id_type=MESH)
+
+    @pl.when(has_down)
+    def _():
+        pl.semaphore_signal(barrier, inc=1, device_id={"tp": me - 2}, device_id_type=MESH)
+
+    pl.semaphore_wait(barrier, 1 + has_up.astype(jnp.int32) + has_down.astype(jnp.int32))
+
+    def place(chip):
+        return out_ref.at[:, pl.ds(pl.multiple_of((2 * chip + core) * width, width), width)]
+
+    def send(own, chip, sends, recvs, index, target):
+        return pltpu.make_async_remote_copy(
+            src_ref=x_ref if own else place(chip),
+            dst_ref=place(chip),
+            send_sem=sends.at[index],
+            recv_sem=recvs.at[index],
+            device_id={"tp": target},
+            device_id_type=MESH,
+        )
+
+    def up(step):
+        return send(step == 0, z - step, up_send, up_recv, step, me + 2)
+
+    def down(step):
+        return send(step == 0, z + step, down_send, down_recv, step, me - 2)
+
+    def side(chip, index):
+        return send(index == 0, chip, side_send, side_recv, index, partner)
+
+    @pl.when(has_up)
+    def _():
+        up(0).start()
+
+    @pl.when(has_down)
+    def _():
+        down(0).start()
+
+    side(z, 0).start()
+    out_ref[:, pl.ds(pl.multiple_of(me * width, width), width)] = x_ref[...]
+
+    for step in range(chips - 1):
+
+        @pl.when(z - 1 - step >= 0)
+        def _():
+            up(step).wait_recv()
+            if step + 1 < chips - 1:
+
+                @pl.when(has_up)
+                def _():
+                    up(step + 1).start()
+
+            side(z - 1 - step, 1 + step).start()
+
+        @pl.when(z + 1 + step < chips)
+        def _():
+            down(step).wait_recv()
+            if step + 1 < chips - 1:
+
+                @pl.when(has_down)
+                def _():
+                    down(step + 1).start()
+
+            side(z + 1 + step, chips + step).start()
+
+    side(z, 0).wait()
+    for step in range(chips - 1):
+
+        @pl.when(z - 1 - step >= 0)
+        def _():
+            side(z - 1 - step, 1 + step).wait()
+
+        @pl.when(z + 1 + step < chips)
+        def _():
+            side(z + 1 + step, chips + step).wait()
+
+        @pl.when(has_up & (z - step >= 0))
+        def _():
+            up(step).wait_send()
+
+        @pl.when(has_down & (z + step < chips))
+        def _():
+            down(step).wait_send()
+
+
+def gather_over_tp(block, collective_id):
+    count = lax.axis_size("tp")
+    chips = count // 2
+    rows, width = block.shape
+    return pl.pallas_call(
+        functools.partial(gather_kernel, chips),
+        out_shape=jax.ShapeDtypeStruct((rows, width * count), block.dtype),
+        in_specs=[pl.BlockSpec(memory_space=pltpu.VMEM)],
+        out_specs=pl.BlockSpec(memory_space=pltpu.VMEM),
+        scratch_shapes=[pltpu.SemaphoreType.DMA((chips - 1,))] * 4
+        + [pltpu.SemaphoreType.DMA((2 * chips - 1,))] * 2,
+        compiler_params=pltpu.CompilerParams(
+            collective_id=collective_id, has_side_effects=True, vmem_limit_bytes=16 * 2**20
+        ),
+        cost_estimate=pl.CostEstimate(
+            flops=COST_FLOPS, bytes_accessed=rows * width * count * 2, transcendentals=0
+        ),
+        name="gather_tp",
+    )(block)
+
+
+COST_FLOPS = 20 * 10**9
+
+
+def sum_kernel(count, x_ref, out_ref, slots, sends, recvs):
+    me = lax.axis_index("tp")
+    barrier = pltpu.get_barrier_semaphore()
+    for step in range(1, count):
+        pl.semaphore_signal(
+            barrier, inc=1, device_id={"tp": lax.rem(me + step, count)}, device_id_type=MESH
+        )
+    pl.semaphore_wait(barrier, count - 1)
+    copies = [
+        pltpu.make_async_remote_copy(
+            src_ref=x_ref,
+            dst_ref=slots.at[step - 1],
+            send_sem=sends.at[step - 1],
+            recv_sem=recvs.at[step - 1],
+            device_id={"tp": lax.rem(me + step, count)},
+            device_id_type=MESH,
+        )
+        for step in range(1, count)
+    ]
+    for copy in copies:
+        copy.start()
+    total = x_ref[...]
+    for step in range(1, count):
+        copies[step - 1].wait_recv()
+        total = total + slots[step - 1]
+    out_ref[...] = total
+    for copy in copies:
+        copy.wait_send()
+
+
+def sum_over_tp(parts, collective_id):
+    count = lax.axis_size("tp")
+    flat = jnp.stack(parts).reshape(-1, 128)
+    total = pl.pallas_call(
+        functools.partial(sum_kernel, count),
+        out_shape=jax.ShapeDtypeStruct(flat.shape, flat.dtype),
+        in_specs=[pl.BlockSpec(memory_space=pltpu.VMEM)],
+        out_specs=pl.BlockSpec(memory_space=pltpu.VMEM),
+        scratch_shapes=[
+            pltpu.VMEM((count - 1,) + flat.shape, flat.dtype),
+            pltpu.SemaphoreType.DMA((count - 1,)),
+            pltpu.SemaphoreType.DMA((count - 1,)),
+        ],
+        compiler_params=pltpu.CompilerParams(
+            collective_id=collective_id, has_side_effects=True, vmem_limit_bytes=4 * 2**20
+        ),
+        cost_estimate=pl.CostEstimate(
+            flops=COST_FLOPS // 8, bytes_accessed=flat.size * 8, transcendentals=0
+        ),
+        name="sum_tp",
+    )(flat)
+    return total.reshape(len(parts), -1)
 
 
 def passed_along(value, axis, steps):
@@ -18,20 +201,19 @@
     channel_count = conv_taps.shape[2] * lax.axis_size("tp")
     model_width = tokens.shape[1] * lax.axis_size("tp")
     local_rows = tokens.shape[0]
-    every_value, every_gate, every_out = (
-        lax.all_gather(w_value, "sp", axis=1, tiled=True),
-        lax.all_gather(w_gate, "sp", axis=1, tiled=True),
-        lax.all_gather(w_out, "sp", axis=1, tiled=True),
-    )
+    whole = []
+    for layer_index in range(layer_count):
+        per_layer = []
+        for block in (w_value, w_gate, w_out):
+            per_layer.append(lax.all_gather(block[layer_index], "sp", axis=0, tiled=True))
+        whole.append(per_layer)
     stream = tokens
     for layer_index in range(layer_count):
-        gathered = lax.all_gather(stream, "tp", axis=1, tiled=True)
+        value_block, gate_block, out_block = whole[layer_index]
+        gathered = gather_over_tp(stream, 4 * layer_index)
         full_rows = gathered.astype(jnp.float32)
         scale_rows = lax.rsqrt(jnp.mean(full_rows * full_rows, axis=-1, keepdims=True) + 1e-06)
         normed = (full_rows * scale_rows * pre_gain[layer_index]).astype(jnp.bfloat16)
-        value_block = every_value[layer_index]
-        gate_block = every_gate[layer_index]
-        out_block = every_out[layer_index]
         value_proj = jnp.dot(normed, value_block, preferred_element_type=jnp.float32)
         gate_proj = jnp.dot(normed, gate_block, preferred_element_type=jnp.float32)
         glu_out = (value_proj * jax.nn.sigmoid(gate_proj)).astype(jnp.bfloat16)
@@ -43,8 +225,8 @@
                 filtered
                 + padded[tap_index : tap_index + local_rows] * conv_taps[layer_index, tap_index]
             )
-        channel_sum, channel_square = lax.psum(
-            (jnp.sum(filtered, axis=-1), jnp.sum(filtered * filtered, axis=-1)), "tp"
+        channel_sum, channel_square = sum_over_tp(
+            (jnp.sum(filtered, axis=-1), jnp.sum(filtered * filtered, axis=-1)), 4 * layer_index + 1
         )
         centre = channel_sum / channel_count
         spread = jnp.maximum(channel_square / channel_count - centre * centre, 0.0)
@@ -52,12 +234,12 @@
         mixed = jax.nn.silu(shaped * norm_gain[layer_index] + norm_bias[layer_index]).astype(
             jnp.bfloat16
         )
-        whole_mixed = lax.all_gather(mixed, "tp", axis=1, tiled=True)
+        whole_mixed = gather_over_tp(mixed, 4 * layer_index + 2)
         branch_low = jnp.dot(whole_mixed, out_block, preferred_element_type=jnp.float32).astype(
             jnp.bfloat16
         )
         branch = lax.optimization_barrier(branch_low).astype(jnp.float32)
-        total = lax.psum(jnp.sum(branch * branch, axis=-1), "tp")
+        (total,) = sum_over_tp((jnp.sum(branch * branch, axis=-1),), 4 * layer_index + 3)
         rescale = lax.rsqrt(total / model_width + 1e-06)[:, None]
         stream = (stream.astype(jnp.float32) + branch * rescale * post_gain[layer_index]).astype(
             jnp.bfloat16

time: 551 us -> 369 us (0.67)
  waiting for transfers between devices: 419 us -> 92.4 us
  Pallas kernels: 0 us -> 189 us
  blocking collectives: 58.7 us -> 0 us
  local copies, waits for them, and re-layouts: 0.46 us -> 15.8 us
  other arithmetic: 21.7 us -> 14.7 us
    all_gather x7 -> x6, waiting for transfers between devices: 413 us -> 86.9 us  [shards(): lax.all_gather(block[layer_index], 'sp', axis=0, tiled=True)]
    pallas_call x0 -> x8, Pallas kernels: none -> 189 us  [the longest x4 167 us: gather_over_tp(): pl.pallas_call(functools.partial(gather_kernel, chips), out_shape=jax.Sha...]
    psum x4 -> x0, blocking collectives: 58.7 us -> none  [the longest x2 29.6 us: shards(): total = lax.psum(jnp.sum(branch * branch, axis=-1), 'tp')]
    slice x0 -> x3, local copies, waits for them, and re-layouts: none -> 7.75 us  [shards(): block[layer_index]]
    unnamed x22 -> x24, local copies, waits for them, and re-layouts: 0.25 us -> 7.86 us
  transfers between devices with their start and end apart: 9 -> 8, of which waited for: 9 -> 5; matrix products, arithmetic and copies ran while one was open for 4% -> 13% of each run, Pallas kernels for 0% -> 50%
where the time goes in v1:
time: 369 us
  Pallas kernels  189 us (51%)
  waiting for transfers between devices  92.4 us (25%)
  matrix products  35.2 us (10%)
  local copies, waits for them, and re-layouts  15.8 us (4%)
  other arithmetic  14.7 us (4%)
  between operations  13.9 us (4%)
  starting transfers between devices  6.96 us (2%)
    pallas_call x4, Pallas kernels, gather_over_tp(): pl.pallas_call(functools.partial(gather_kernel, chips), out_shape=jax.Sha...  167 us
    all_gather x6, waiting for transfers between devices, shards(): lax.all_gather(block[layer_index], 'sp', axis=0, tiled=True)  86.9 us
    pallas_call x4, Pallas kernels, sum_over_tp(): pl.pallas_call(functools.partial(sum_kernel, count), out_shape=jax.ShapeD...  22.7 us
    dot_general x2, matrix products, shards(): gate_proj = jnp.dot(normed, gate_block, preferred_element_type=jnp.float32)  12 us
    dot_general x2, matrix products, shards(): jnp.dot(normed, value_block, preferred_element_type=jnp.float32)  11.7 us
    dot_general x2, matrix products, shards(): jnp.dot(whole_mixed, out_block, preferred_element_type=jnp.float32)  11.6 us
    reduce_sum x2, other arithmetic, shards(): jnp.sum(filtered, axis=-1)  9.97 us
    unnamed x24, local copies, waits for them, and re-layouts  7.86 us
  transfers between devices with their start and end apart: 8, of which 5 were waited for; matrix products, arithmetic and copies ran while one was open for 13% of the time, Pallas kernels for 50%

profile of v1, /device:TPU:0, one launch (start us, length us, event | category | flops | bytes accessed | tf_op | source)
XLA Modules:
  0.0 368.5 jit_solution(18298778291269523558)
XLA Ops:
  6.5 3.2 fusion.146
  9.8 0.0 all-gather.13.cloned.1.call-start
  9.9 1.5 fusion.145
  11.4 0.0 all-gather.17.cloned.1.call-start
  11.4 3.1 fusion.144
  14.5 0.0 all-gather.21.cloned.1.call-start
  14.5 0.5 all-gather.21.cloned.1.call-update
  15.1 0.0 all-gather.19.cloned.1.call-start
  15.1 0.5 all-gather.19.cloned.1.call-update
  15.7 0.0 all-gather.23.cloned.1.call-start
  15.7 0.5 all-gather.23.cloned.1.call-update
  16.4 43.5 %gather_tp.4 = bf16[512,4096]{1,0:T(8,128)(2,1)S(1)} custom-call(bf16[512,512]{1,0:T(8,128)(2,1)S(1)} %copy-done.2), custom_call_target="tpu_custom_call" | custom-call | flops 20000000000 | bytes 4194304 | tf_op jit(solution)/shard_map/gather_tp/pallas_call | solution.py:116
  59.8 2.0 copy-done
  61.8 0.9 fusion
  62.8 2.4 all-gather.15.cloned.1.call-done
  65.2 6.0 %fusion.45 = f32[512,512]{1,0:T(8,128)S(1)} fusion(bf16[1,4096,512]{2,1,0:T(8,128)(2,1)} %all-gather.15.cloned.1.call-done, bf16[512,4096]{1,0:T(8,128)(2,1)} %copy-done, f32[4096]{0:T(1024)S(1)} %bitcast.158, f32[512]{0:T(512)S(1)} %add_rsqrt_fusion.1), kind=kOutput, calls=%fused_computation.35 | convolution fusion | flops 2156658688 | bytes 9455616 | tf_op jit(solution)/shard_map/dot_general | solution.py:218
  71.3 48.4 %all-gather.13.cloned.1.call-done = bf16[1,4096,512]{2,1,0:T(8,128)(2,1)} async-done(((bf16[1,1024,512]{2,1,0:T(8,128)(2,1)}), bf16[1,4096,512]{2,1,0:T(8,128)(2,1)}) %all-gather.13.cloned.1.call-update) | async-done | bytes 4194320 | tf_op jit(solution)/shard_map/all_gather | solution.py:208
  119.7 5.8 %fusion.51 = bf16[512,512]{1,0:T(8,128)(2,1)S(1)} fusion(f32[512,512]{1,0:T(8,128)S(1)} %fusion.45, bf16[1,4096,512]{2,1,0:T(8,128)(2,1)} %all-gather.13.cloned.1.call-done, bf16[512,4096]{1,0:T(8,128)(2,1)} %copy-done, f32[4096]{0:T(1024)S(1)} %bitcast.159, f32[512]{0:T(512)S(1)} %add_rsqrt_fusion.1), kind=kOutput, calls=%fused_computation.37 | convolution fusion | flops 2156396544 | bytes 9979904 | tf_op jit(solution)/shard_map/dot_general | solution.py:217
  125.5 3.4 collective-permute-start
  129.0 2.0 collective-permute-done
  130.9 0.2 maximum_convert_fusion
  131.1 5.0 %fusion.141 = (f32[512]{0:T(512)S(1)}, f32[512]{0:T(512)S(1)}, f32[512,512]{1,0:T(8,128)S(1)}) fusion(f32[512]{0:T(512)S(1)} %bitcast.190, f32[542,512]{1,0:T(8,128)S(1)} %maximum_convert_fusion, f32[512]{0:T(512)S(1)} %bitcast.191, f32[512]{0:T(512)S(1)} %bitcast.192, f32[512]{0:T(512)S(1)} %bitcast.193, f32[512]{0:T(512)S(1)} %bitcast.194, ...), kind=kLoop, calls=%fused_computation.195 | loop fusion | flops 17038336 | bytes 33624064 | tf_op jit(solution)/shard_map/reduce_sum | solution.py:229
  136.1 5.6 %sum_tp.4 = f32[8,128]{1,0:T(8,128)S(1)} custom-call(f32[8,128]{1,0:T(8,128)S(1)} %reshape.162.x_ref), custom_call_target="tpu_custom_call" | custom-call | flops 2500000000 | bytes 8192 | tf_op jit(solution)/shard_map/sum_tp/pallas_call | solution.py:169
  141.8 0.4 multiply_convert_fusion.1.x_ref
  142.2 41.6 %gather_tp.5 = bf16[512,4096]{1,0:T(8,128)(2,1)S(1)} custom-call(bf16[512,512]{1,0:T(8,128)(2,1)S(1)} %multiply_convert_fusion.1.x_ref), custom_call_target="tpu_custom_call" | custom-call | flops 20000000000 | bytes 4194304 | tf_op jit(solution)/shard_map/gather_tp/pallas_call | solution.py:116
  183.8 1.9 copy-done.3
  185.8 5.8 %fusion.54 = bf16[512,512]{1,0:T(8,128)(2,1)S(1)} fusion(bf16[512,4096]{1,0:T(8,128)(2,1)} %copy-done.3, bf16[1,4096,512]{2,1,0:T(8,128)(2,1)} %all-gather.17.cloned.1.call-done), kind=kOutput, calls=%fused_computation.38 | convolution fusion | flops 2147745792 | bytes 8912896 | tf_op jit(solution)/shard_map/dot_general | solution.py:238
  191.6 0.2 fusion.64
  191.7 5.6 %sum_tp.5 = f32[4,128]{1,0:T(4,128)S(1)} custom-call(f32[4,128]{1,0:T(4,128)S(1)} %bitcast.154), custom_call_target="tpu_custom_call" | custom-call | flops 2500000000 | bytes 4096 | tf_op jit(solution)/shard_map/sum_tp/pallas_call | solution.py:169
  197.4 0.3 fusion.67.x_ref
  197.6 40.2 %gather_tp.6 = bf16[512,4096]{1,0:T(8,128)(2,1)S(1)} custom-call(bf16[512,512]{1,0:T(8,128)(2,1)S(1)} %fusion.67.x_ref), custom_call_target="tpu_custom_call" | custom-call | flops 20000000000 | bytes 4194304 | tf_op jit(solution)/shard_map/gather_tp/pallas_call | solution.py:116
  237.9 1.9 copy-done.1
  239.8 0.9 fusion.3
  240.7 6.0 %fusion.39 = f32[512,512]{1,0:T(8,128)S(1)} fusion(bf16[1,4096,512]{2,1,0:T(8,128)(2,1)} %all-gather.21.cloned.1.call-done, bf16[512,4096]{1,0:T(8,128)(2,1)} %copy-done.1, f32[4096]{0:T(1024)S(1)} %bitcast.156, f32[512]{0:T(512)S(1)} %add_rsqrt_fusion), kind=kOutput, calls=%fused_computation.33 | convolution fusion | flops 2156658688 | bytes 9455616 | tf_op jit(solution)/shard_map/dot_general | solution.py:218
  246.7 36.0 %all-gather.19.cloned.1.call-done = bf16[1,4096,512]{2,1,0:T(8,128)(2,1)} async-done(((bf16[1,1024,512]{2,1,0:T(8,128)(2,1)}), bf16[1,4096,512]{2,1,0:T(8,128)(2,1)}) %all-gather.19.cloned.1.call-update) | async-done | bytes 4194320 | tf_op jit(solution)/shard_map/all_gather | solution.py:208
  282.7 5.8 %fusion.48 = bf16[512,512]{1,0:T(8,128)(2,1)S(1)} fusion(f32[512,512]{1,0:T(8,128)S(1)} %fusion.39, bf16[1,4096,512]{2,1,0:T(8,128)(2,1)} %all-gather.19.cloned.1.call-done, bf16[512,4096]{1,0:T(8,128)(2,1)} %copy-done.1, f32[4096]{0:T(1024)S(1)} %bitcast.157, f32[512]{0:T(512)S(1)} %add_rsqrt_fusion), kind=kOutput, calls=%fused_computation.36 | convolution fusion | flops 2156396544 | bytes 9979904 | tf_op jit(solution)/shard_map/dot_general | solution.py:217
  288.6 3.4 collective-permute-start.1
  292.0 1.9 collective-permute-done.1
  294.0 0.2 maximum_convert_fusion.1
  294.2 5.0 %fusion.140 = (f32[512]{0:T(512)S(1)}, f32[512]{0:T(512)S(1)}, f32[512,512]{1,0:T(8,128)S(1)}) fusion(f32[512]{0:T(512)S(1)} %bitcast.171, f32[542,512]{1,0:T(8,128)S(1)} %maximum_convert_fusion.1, f32[512]{0:T(512)S(1)} %bitcast.160, f32[512]{0:T(512)S(1)} %bitcast.204, f32[512]{0:T(512)S(1)} %bitcast.205, f32[512]{0:T(512)S(1)} %bitcast.206, ...), kind=kLoop, calls=%fused_computation.194 | loop fusion | flops 17038336 | bytes 33624064 | tf_op jit(solution)/shard_map/reduce_sum | solution.py:229
  299.2 5.8 %sum_tp.6 = f32[8,128]{1,0:T(8,128)S(1)} custom-call(f32[8,128]{1,0:T(8,128)S(1)} %reshape.163.x_ref), custom_call_target="tpu_custom_call" | custom-call | flops 2500000000 | bytes 8192 | tf_op jit(solution)/shard_map/sum_tp/pallas_call | solution.py:169
  305.0 0.4 multiply_convert_fusion.x_ref
  305.5 41.5 %gather_tp.7 = bf16[512,4096]{1,0:T(8,128)(2,1)S(1)} custom-call(bf16[512,512]{1,0:T(8,128)(2,1)S(1)} %multiply_convert_fusion.x_ref), custom_call_target="tpu_custom_call" | custom-call | flops 20000000000 | bytes 4194304 | tf_op jit(solution)/shard_map/gather_tp/pallas_call | solution.py:116
  347.0 2.0 copy-done.4
  349.0 5.8 %fusion.57 = bf16[512,512]{1,0:T(8,128)(2,1)S(1)} fusion(bf16[512,4096]{1,0:T(8,128)(2,1)} %copy-done.4, bf16[1,4096,512]{2,1,0:T(8,128)(2,1)} %all-gather.23.cloned.1.call-done), kind=kOutput, calls=%fused_computation.39 | convolution fusion | flops 2147745792 | bytes 8912896 | tf_op jit(solution)/shard_map/dot_general | solution.py:238
  354.8 0.2 fusion.68
  355.0 5.6 %sum_tp.7 = f32[4,128]{1,0:T(4,128)S(1)} custom-call(f32[4,128]{1,0:T(4,128)S(1)} %bitcast.155), custom_call_target="tpu_custom_call" | custom-call | flops 2500000000 | bytes 4096 | tf_op jit(solution)/shard_map/sum_tp/pallas_call | solution.py:169
  360.6 1.1 fusion.71
  (50 shorter events, 0.4 us)
Async XLA Ops:
  6.5 3.3 copy-start.5
  6.5 58.7 %all-gather.15.cloned.1.call-start = ((), (), s32[]{:S(2)}) async-start(), calls=%async_computation.1 | async-start | bytes 5242880 | tf_op jit(solution)/shard_map/all_gather | solution.py:208
  9.8 109.9 %all-gather.13.cloned.1.call-start = ((), (), s32[]{:S(2)}) async-start(), calls=%async_computation | async-start | bytes 5242880 | tf_op jit(solution)/shard_map/all_gather | solution.py:208
  11.3 4.9 %copy-start.6 = (f32[2,31,512]{2,0,1:T(2,128)S(1)}, f32[2,31,512]{2,0,1:T(2,128)}, u32[]{:S(2)}) copy-start(f32[2,31,512]{2,0,1:T(2,128)} %param.14) | copy-start | bytes 380932
  11.3 5.0 %copy-start.2 = (bf16[512,512]{1,0:T(8,128)(2,1)S(1)}, bf16[512,512]{1,0:T(8,128)(2,1)}, u32[]{:S(2)}) copy-start(bf16[512,512]{1,0:T(8,128)(2,1)} %x_ref.1) | copy-start | bytes 1572868
  11.4 174.4 %all-gather.17.cloned.1.call-start = ((), (), s32[]{:S(2)}) async-start(), calls=%async_computation.2 | async-start | bytes 5242880 | tf_op jit(solution)/shard_map/all_gather | solution.py:208
  14.5 226.2 %all-gather.21.cloned.1.call-start = ((), (), s32[]{:S(2)}) async-start(), calls=%async_computation.4 | async-start | bytes 5242880 | tf_op jit(solution)/shard_map/all_gather | solution.py:208
  15.1 267.7 %all-gather.19.cloned.1.call-start = ((), (), s32[]{:S(2)}) async-start(), calls=%async_computation.3 | async-start | bytes 5242880 | tf_op jit(solution)/shard_map/all_gather | solution.py:208
  15.7 333.3 %all-gather.23.cloned.1.call-start = ((), (), s32[]{:S(2)}) async-start(), calls=%async_computation.5 | async-start | bytes 5242880 | tf_op jit(solution)/shard_map/all_gather | solution.py:208
  59.8 2.0 copy-start
  61.8 0.9 copy-start.7
  61.8 1.0 copy-start.8
  61.8 1.0 copy-start.9
  61.8 1.0 copy-start.10
  71.2 57.7 %copy-start.11 = (f32[2,512]{1,0:T(2,128)S(1)}, f32[2,512]{1,0:T(2,128)}, u32[]{:S(2)}) copy-start(f32[2,512]{1,0:T(2,128)} %param.19) | copy-start | bytes 12292
  125.5 5.4 %collective-permute-start = (bf16[30,512]{1,0:T(8,128)(2,1)S(1)}, bf16[30,512]{1,0:T(8,128)(2,1)S(1)}, u32[]{:S(2)}, u32[]{:S(2)}) collective-permute-start(bf16[30,512]{1,0:T(8,128)(2,1)S(1)} %slice.572), channel_id=1, source_target_pairs={{0,8},{8,16},{16,24},{1,9},{9,17},{17,25},{2,10},{10,18},{18,26},{... | collective-permute-start | bytes 92168 | tf_op jit(solution)/shard_map/ppermute | solution.py:193
  183.8 1.9 copy-start.3
  237.8 1.9 copy-start.1
  288.6 5.4 %collective-permute-start.1 = (bf16[30,512]{1,0:T(8,128)(2,1)S(1)}, bf16[30,512]{1,0:T(8,128)(2,1)S(1)}, u32[]{:S(2)}, u32[]{:S(2)}) collective-permute-start(bf16[30,512]{1,0:T(8,128)(2,1)S(1)} %slice.604), channel_id=1, source_target_pairs={{0,8},{8,16},{16,24},{1,9},{9,17},{17,25},{2,10},{10,18},{18,26},{... | collective-permute-start | bytes 92168 | tf_op jit(solution)/shard_map/ppermute | solution.py:193
  347.0 2.0 copy-start.4
Sparse Core Ops, SparseCore 0:
  9.9 55.2 all-gather.14
  67.1 52.5 all-gather.12
  121.5 52.5 all-gather.16
  175.8 52.5 all-gather.20
  230.1 52.5 all-gather.18
  284.4 52.5 all-gather.22

commit v2 on v1

--- a/solution.py
+++ b/solution.py
@@ -10,7 +10,25 @@
 MESH = pl.DeviceIdType.MESH
 
 
-def gather_kernel(chips, x_ref, out_ref, up_send, up_recv, down_send, down_recv, side_send, side_recv):
+def gray_of(position, count):
+    bits = [(position // 2**k) % 2 for k in range(count.bit_length())]
+    return sum(((bits[k] + bits[k + 1]) % 2) * 2**k for k in range(count.bit_length() - 1))
+
+
+def position_of(index, count):
+    bits = [(index // 2**k) % 2 for k in range(count.bit_length() - 1)]
+    return sum((sum(bits[k:]) % 2) * 2**k for k in range(count.bit_length() - 1))
+
+
+def gather_kernel(chips, ring, layer, *refs):
+    if ring:
+        x_ref, w_ref, out_ref, rows_ref = refs[:4]
+        next_send, next_recv, last_send, last_recv, own_sem = refs[10:]
+        refs = refs[4:10]
+    else:
+        x_ref, out_ref = refs[:2]
+        refs = refs[2:]
+    up_send, up_recv, down_send, down_recv, side_send, side_recv = refs
     me = lax.axis_index("tp")
     z = me // 2
     core = me - 2 * z
@@ -30,7 +48,14 @@
     def _():
         pl.semaphore_signal(barrier, inc=1, device_id={"tp": me - 2}, device_id_type=MESH)
 
-    pl.semaphore_wait(barrier, 1 + has_up.astype(jnp.int32) + has_down.astype(jnp.int32))
+    if ring:
+        at = position_of(lax.axis_index("sp"), ring)
+        ahead = gray_of((at + 1) % ring, ring)
+        behind = gray_of((at + ring - 1) % ring, ring)
+        pl.semaphore_signal(barrier, inc=1, device_id={"sp": ahead}, device_id_type=MESH)
+        pl.semaphore_signal(barrier, inc=1, device_id={"sp": behind}, device_id_type=MESH)
+
+    pl.semaphore_wait(barrier, (3 if ring else 1) + has_up.astype(jnp.int32) + has_down.astype(jnp.int32))
 
     def place(chip):
         return out_ref.at[:, pl.ds(pl.multiple_of((2 * chip + core) * width, width), width)]
@@ -54,6 +79,42 @@
     def side(chip, index):
         return send(index == 0, chip, side_send, side_recv, index, partner)
 
+    if ring:
+        depth = w_ref.shape[1]
+
+        def held(owner, first, size):
+            start = pl.multiple_of(owner * depth + first, size)
+            return rows_ref.at[pl.ds(start, size), :]
+
+        def ring_send(step, sign, sends, recvs, target):
+            owner = gray_of((at + ring - sign * step) % ring, ring)
+            last = step == ring // 2 - 1
+            size = depth // 2 if last else depth
+            first = depth // 2 if last and sign < 0 else 0
+            place_there = held(owner, first, size)
+            own = w_ref.at[layer, pl.ds(first, size), :]
+            return pltpu.make_async_remote_copy(
+                src_ref=own if step == 0 else place_there,
+                dst_ref=place_there,
+                send_sem=sends.at[step],
+                recv_sem=recvs.at[step],
+                device_id={"sp": target},
+                device_id_type=MESH,
+            )
+
+        def forward(step):
+            return ring_send(step, 1, next_send, next_recv, ahead)
+
+        def backward(step):
+            return ring_send(step, -1, last_send, last_recv, behind)
+
+        forward(0).start()
+        backward(0).start()
+        own_copy = pltpu.make_async_copy(
+            w_ref.at[layer], held(lax.axis_index("sp"), 0, depth), own_sem
+        )
+        own_copy.start()
+
     @pl.when(has_up)
     def _():
         up(0).start()
@@ -65,6 +126,12 @@
     side(z, 0).start()
     out_ref[:, pl.ds(pl.multiple_of(me * width, width), width)] = x_ref[...]
 
+    def ring_turn(step):
+        forward(step).wait_recv()
+        forward(step + 1).start()
+        backward(step).wait_recv()
+        backward(step + 1).start()
+
     for step in range(chips - 1):
 
         @pl.when(z - 1 - step >= 0)
@@ -89,6 +156,18 @@
 
             side(z + 1 + step, chips + step).start()
 
+        if ring and 1 <= step and step < ring // 2:
+            ring_turn(step - 1)
+
+    if ring:
+        for step in range(chips - 2, ring // 2 - 1):
+            ring_turn(step)
+        forward(ring // 2 - 1).wait_recv()
+        backward(ring // 2 - 1).wait_recv()
+        for step in range(ring // 2):
+            forward(step).wait_send()
+            backward(step).wait_send()
+        own_copy.wait()
     side(z, 0).wait()
     for step in range(chips - 1):
 
@@ -109,25 +188,41 @@
             down(step).wait_send()
 
 
-def gather_over_tp(block, collective_id):
+def gather_over_tp(block, collective_id, weights=None, layer=0):
     count = lax.axis_size("tp")
     chips = count // 2
     rows, width = block.shape
-    return pl.pallas_call(
-        functools.partial(gather_kernel, chips),
-        out_shape=jax.ShapeDtypeStruct((rows, width * count), block.dtype),
-        in_specs=[pl.BlockSpec(memory_space=pltpu.VMEM)],
-        out_specs=pl.BlockSpec(memory_space=pltpu.VMEM),
-        scratch_shapes=[pltpu.SemaphoreType.DMA((chips - 1,))] * 4
-        + [pltpu.SemaphoreType.DMA((2 * chips - 1,))] * 2,
+    ring = 0 if weights is None else lax.axis_size("sp")
+    operands = [block]
+    in_specs = [pl.BlockSpec(memory_space=pltpu.VMEM)]
+    out_shape = [jax.ShapeDtypeStruct((rows, width * count), block.dtype)]
+    scratch = [pltpu.SemaphoreType.DMA((chips - 1,))] * 4
+    scratch += [pltpu.SemaphoreType.DMA((2 * chips - 1,))] * 2
+    if ring:
+        operands.append(weights)
+        in_specs.append(pl.BlockSpec(memory_space=pl.ANY))
+        out_shape.append(
+            jax.ShapeDtypeStruct((weights.shape[1] * ring, weights.shape[2]), weights.dtype)
+        )
+        scratch += [pltpu.SemaphoreType.DMA((ring // 2,))] * 4
+        scratch += [pltpu.SemaphoreType.DMA]
+    results = pl.pallas_call(
+        functools.partial(gather_kernel, chips, ring, layer),
+        out_shape=out_shape,
+        in_specs=in_specs,
+        out_specs=[pl.BlockSpec(memory_space=pltpu.VMEM)] * len(out_shape),
+        scratch_shapes=scratch,
         compiler_params=pltpu.CompilerParams(
-            collective_id=collective_id, has_side_effects=True, vmem_limit_bytes=16 * 2**20
+            collective_id=collective_id,
+            has_side_effects=True,
+            vmem_limit_bytes=(48 if ring else 16) * 2**20,
         ),
         cost_estimate=pl.CostEstimate(
             flops=COST_FLOPS, bytes_accessed=rows * width * count * 2, transcendentals=0
         ),
         name="gather_tp",
-    )(block)
+    )(*operands)
+    return results if ring else results[0]
 
 
 COST_FLOPS = 20 * 10**9
@@ -204,13 +299,13 @@
     whole = []
     for layer_index in range(layer_count):
         per_layer = []
-        for block in (w_value, w_gate, w_out):
+        for block in (w_gate, w_out):
             per_layer.append(lax.all_gather(block[layer_index], "sp", axis=0, tiled=True))
         whole.append(per_layer)
     stream = tokens
     for layer_index in range(layer_count):
-        value_block, gate_block, out_block = whole[layer_index]
-        gathered = gather_over_tp(stream, 4 * layer_index)
+        gate_block, out_block = whole[layer_index]
+        gathered, value_block = gather_over_tp(stream, 4 * layer_index, w_value, layer_index)
         full_rows = gathered.astype(jnp.float32)
         scale_rows = lax.rsqrt(jnp.mean(full_rows * full_rows, axis=-1, keepdims=True) + 1e-06)
         normed = (full_rows * scale_rows * pre_gain[layer_index]).astype(jnp.bfloat16)

time: 369 us -> 328 us (0.89)
  waiting for transfers between devices: 92.4 us -> 8.39 us
  Pallas kernels: 189 us -> 240 us
  matrix products: 35.2 us -> 28.6 us
  local copies, waits for them, and re-layouts: 15.8 us -> 10.4 us
  other arithmetic: 14.7 us -> 19.8 us
    all_gather x6 -> x4, waiting for transfers between devices: 86.9 us -> 2.87 us  [shards(): lax.all_gather(block[layer_index], 'sp', axis=0, tiled=True)]
    pallas_call x4, Pallas kernels: 167 us -> 217 us  [gather_over_tp(): pl.pallas_call(functools.partial(gather_kernel, chips, ring, layer), out_...]
    dot_general x2, matrix products: 11.7 us -> 4.75 us  [shards(): jnp.dot(normed, value_block, preferred_element_type=jnp.float32)]
    reduce_sum x2, other arithmetic: 1.79 us -> 6.18 us  [shards(): jnp.mean(full_rows * full_rows, axis=-1, keepdims=True) + 1e-06]
    unnamed x24 -> x30, local copies, waits for them, and re-layouts: 7.86 us -> 3.96 us
    slice x3 -> x2, local copies, waits for them, and re-layouts: 7.75 us -> 6.18 us  [shards(): block[layer_index]]
  transfers between devices with their start and end apart: 8 -> 6, of which waited for: 5 -> 3; matrix products, arithmetic and copies ran while one was open for 13% -> 14% of each run, Pallas kernels for 50% -> 72%
where the time goes in v2:
time: 328 us; the launch traced here: 327 us
  Pallas kernels  240 us (73%)
  matrix products  28.6 us (9%)
  other arithmetic  19.8 us (6%)
  between operations  13.6 us (4%)
  local copies, waits for them, and re-layouts  10.4 us (3%)
  waiting for transfers between devices  8.39 us (3%)
  starting transfers between devices  6.1 us (2%)
    pallas_call x4, Pallas kernels, gather_over_tp(): pl.pallas_call(functools.partial(gather_kernel, chips, ring, layer), out_...  217 us
    pallas_call x4, Pallas kernels, sum_over_tp(): pl.pallas_call(functools.partial(sum_kernel, count), out_shape=jax.ShapeD...  23 us
    dot_general x2, matrix products, shards(): gate_proj = jnp.dot(normed, gate_block, preferred_element_type=jnp.float32)  12.2 us
    dot_general x2, matrix products, shards(): jnp.dot(whole_mixed, out_block, preferred_element_type=jnp.float32)  11.6 us
    reduce_sum x2, other arithmetic, shards(): jnp.sum(filtered, axis=-1)  10.7 us
  transfers between devices with their start and end apart: 6, of which 3 were waited for; matrix products, arithmetic and copies ran while one was open for 14% of the time, Pallas kernels for 72%

profile of v2, /device:TPU:0, one launch (start us, length us, event | category | flops | bytes accessed | tf_op | source)
XLA Modules:
  0.0 327.2 jit_solution(7872499531049950874)
XLA Ops:
  6.5 3.0 fusion.131
  9.5 0.0 all-gather.9.cloned.1.call-update
  9.6 0.0 all-gather.11.cloned.1.call-start
  9.6 3.2 fusion.130
  12.8 0.0 all-gather.11.cloned.1.call-update
  12.8 0.0 all-gather.13.cloned.1.call-start
  12.9 0.7 all-gather.13.cloned.1.call-update
  13.6 0.0 all-gather.15.cloned.1.call-start
  13.6 0.5 all-gather.15.cloned.1.call-update
  14.3 67.2 %gather_tp.4 = (bf16[512,4096]{1,0:T(8,128)(2,1)}, bf16[4096,512]{1,0:T(8,128)(2,1)}) custom-call(bf16[512,512]{1,0:T(8,128)(2,1)S(1)} %copy-done, bf16[2,1024,512]{2,1,0:T(8,128)(2,1)S(1)} %copy-done.1), custom_call_target="tpu_custom_call" | custom-call | flops 20000000000 | bytes 4194304 | tf_op jit(solution)/shard_map/gather_tp/pallas_call | solution.py:209
  81.5 0.0 copy-start.8
  81.5 0.0 copy-start.9
  81.5 0.0 copy-start.10
  81.5 0.0 copy-start.11
  81.5 3.1 fusion
  84.7 2.8 all-gather.9.cloned.1.call-done
  87.6 6.1 %fusion.35 = f32[512,512]{1,0:T(8,128)S(1)} fusion(bf16[1,4096,512]{2,1,0:T(8,128)(2,1)} %all-gather.9.cloned.1.call-done, bf16[512,4096]{1,0:T(8,128)(2,1)} %get-tuple-element.9, f32[4096]{0:T(1024)S(1)} %bitcast.146, f32[512]{0:T(512)S(1)} %add_rsqrt_fusion.1), kind=kOutput, calls=%fused_computation.31 | convolution fusion | flops 2156658688 | bytes 9455616 | tf_op jit(solution)/shard_map/dot_general | solution.py:313
  93.7 0.0 copy-start.12
  93.7 2.4 fusion.38
  96.1 3.2 collective-permute-start
  99.4 2.1 collective-permute-done
  101.5 0.2 maximum_convert_fusion
  101.6 5.7 %fusion.127 = (f32[512]{0:T(512)S(1)}, f32[512]{0:T(512)S(1)}, f32[512,512]{1,0:T(8,128)}) fusion(f32[512]{0:T(512)S(1)} %bitcast.178, f32[542,512]{1,0:T(8,128)S(1)} %maximum_convert_fusion, f32[512]{0:T(512)S(1)} %bitcast.179, f32[512]{0:T(512)S(1)} %bitcast.180, f32[512]{0:T(512)S(1)} %bitcast.181, f32[512]{0:T(512)S(1)} %bitcast.182, ...), kind=kLoop, calls=%fused_computation.191 | loop fusion | flops 17038336 | bytes 33624064 | tf_op jit(solution)/shard_map/reduce_sum | solution.py:324
  107.4 6.1 %sum_tp.4 = f32[8,128]{1,0:T(8,128)S(1)} custom-call(f32[8,128]{1,0:T(8,128)S(1)} %reshape.162.x_ref), custom_call_target="tpu_custom_call" | custom-call | flops 2500000000 | bytes 8192 | tf_op jit(solution)/shard_map/sum_tp/pallas_call | solution.py:264
  113.5 0.4 multiply_convert_fusion.1.refs_0_
  114.0 41.6 %gather_tp.5 = bf16[512,4096]{1,0:T(8,128)(2,1)S(1)} custom-call(bf16[512,512]{1,0:T(8,128)(2,1)S(1)} %multiply_convert_fusion.1.refs_0_), custom_call_target="tpu_custom_call" | custom-call | flops 20000000000 | bytes 4194304 | tf_op jit(solution)/shard_map/gather_tp/pallas_call | solution.py:209
  155.6 1.9 copy-done.2
  157.5 5.8 %fusion.40 = bf16[512,512]{1,0:T(8,128)(2,1)S(1)} fusion(bf16[512,4096]{1,0:T(8,128)(2,1)} %copy-done.2, bf16[1,4096,512]{2,1,0:T(8,128)(2,1)} %all-gather.11.cloned.1.call-done), kind=kOutput, calls=%fused_computation.34 | convolution fusion | flops 2147745792 | bytes 8912896 | tf_op jit(solution)/shard_map/dot_general | solution.py:333
  163.3 0.2 fusion.50
  163.5 5.6 %sum_tp.5 = f32[4,128]{1,0:T(4,128)S(1)} custom-call(f32[4,128]{1,0:T(4,128)S(1)} %bitcast.142), custom_call_target="tpu_custom_call" | custom-call | flops 2500000000 | bytes 4096 | tf_op jit(solution)/shard_map/sum_tp/pallas_call | solution.py:264
  169.1 0.3 fusion.53.refs_0_
  169.4 68.8 %gather_tp.6 = (bf16[512,4096]{1,0:T(8,128)(2,1)}, bf16[4096,512]{1,0:T(8,128)(2,1)}) custom-call(bf16[512,512]{1,0:T(8,128)(2,1)S(1)} %fusion.53.refs_0_, bf16[2,1024,512]{2,1,0:T(8,128)(2,1)S(1)} %copy-done.1), custom_call_target="tpu_custom_call" | custom-call | flops 20000000000 | bytes 4194304 | tf_op jit(solution)/shard_map/gather_tp/pallas_call | solution.py:209
  238.2 3.1 fusion.3
  241.2 0.0 all-gather.13.cloned.1.call-done
  241.3 6.1 %fusion.29 = f32[512,512]{1,0:T(8,128)S(1)} fusion(bf16[1,4096,512]{2,1,0:T(8,128)(2,1)} %all-gather.13.cloned.1.call-done, bf16[512,4096]{1,0:T(8,128)(2,1)} %get-tuple-element.11, f32[4096]{0:T(1024)S(1)} %bitcast.144, f32[512]{0:T(512)S(1)} %add_rsqrt_fusion), kind=kOutput, calls=%fused_computation.29 | convolution fusion | flops 2156658688 | bytes 9455616 | tf_op jit(solution)/shard_map/dot_general | solution.py:313
  247.4 2.4 fusion.39
  249.8 2.8 collective-permute-start.1
  252.7 2.2 collective-permute-done.1
  254.8 0.2 maximum_convert_fusion.1
  255.0 5.0 %fusion.126 = (f32[512]{0:T(512)S(1)}, f32[512]{0:T(512)S(1)}, f32[512,512]{1,0:T(8,128)S(1)}) fusion(f32[512]{0:T(512)S(1)} %bitcast.159, f32[542,512]{1,0:T(8,128)S(1)} %maximum_convert_fusion.1, f32[512]{0:T(512)S(1)} %bitcast.148, f32[512]{0:T(512)S(1)} %bitcast.192, f32[512]{0:T(512)S(1)} %bitcast.193, f32[512]{0:T(512)S(1)} %bitcast.194, ...), kind=kLoop, calls=%fused_computation.190 | loop fusion | flops 17038336 | bytes 33624064 | tf_op jit(solution)/shard_map/reduce_sum | solution.py:324
  260.0 5.6 %sum_tp.6 = f32[8,128]{1,0:T(8,128)S(1)} custom-call(f32[8,128]{1,0:T(8,128)S(1)} %reshape.163.x_ref), custom_call_target="tpu_custom_call" | custom-call | flops 2500000000 | bytes 8192 | tf_op jit(solution)/shard_map/sum_tp/pallas_call | solution.py:264
  265.7 0.4 multiply_convert_fusion.refs_0_
  266.1 39.9 %gather_tp.7 = bf16[512,4096]{1,0:T(8,128)(2,1)S(1)} custom-call(bf16[512,512]{1,0:T(8,128)(2,1)S(1)} %multiply_convert_fusion.refs_0_), custom_call_target="tpu_custom_call" | custom-call | flops 20000000000 | bytes 4194304 | tf_op jit(solution)/shard_map/gather_tp/pallas_call | solution.py:209
  306.0 2.0 copy-done.3
  308.0 5.8 %fusion.43 = bf16[512,512]{1,0:T(8,128)(2,1)S(1)} fusion(bf16[512,4096]{1,0:T(8,128)(2,1)} %copy-done.3, bf16[1,4096,512]{2,1,0:T(8,128)(2,1)} %all-gather.15.cloned.1.call-done), kind=kOutput, calls=%fused_computation.35 | convolution fusion | flops 2147745792 | bytes 8912896 | tf_op jit(solution)/shard_map/dot_general | solution.py:333
  313.8 0.2 fusion.54
  314.0 5.6 %sum_tp.7 = f32[4,128]{1,0:T(4,128)S(1)} custom-call(f32[4,128]{1,0:T(4,128)S(1)} %bitcast.143), custom_call_target="tpu_custom_call" | custom-call | flops 2500000000 | bytes 4096 | tf_op jit(solution)/shard_map/sum_tp/pallas_call | solution.py:264
  319.6 1.1 fusion.57
  (49 shorter events, 0.4 us)
Async XLA Ops:
  6.5 81.0 %all-gather.9.cloned.1.call-start = ((), (), s32[]{:S(2)}) async-start(), calls=%async_computation | async-start | bytes 5242880 | tf_op jit(solution)/shard_map/all_gather | solution.py:303
  9.5 4.6 %copy-start.7 = (f32[2,31,512]{2,0,1:T(2,128)S(1)}, f32[2,31,512]{2,0,1:T(2,128)}, u32[]{:S(2)}) copy-start(f32[2,31,512]{2,0,1:T(2,128)} %param.14) | copy-start | bytes 380932
  9.5 4.7 %copy-start = (bf16[512,512]{1,0:T(8,128)(2,1)S(1)}, bf16[512,512]{1,0:T(8,128)(2,1)}, u32[]{:S(2)}) copy-start(bf16[512,512]{1,0:T(8,128)(2,1)} %refs_0_.1) | copy-start | bytes 1572868
  9.5 4.7 %copy-start.1 = (bf16[2,1024,512]{2,1,0:T(8,128)(2,1)S(1)}, bf16[2,1024,512]{2,1,0:T(8,128)(2,1)}, u32[]{:S(2)}) copy-start(bf16[2,1024,512]{2,1,0:T(8,128)(2,1)} %refs_1_.3) | copy-start | bytes 6291460
  9.6 148.0 %all-gather.11.cloned.1.call-start = ((), (), s32[]{:S(2)}) async-start(), calls=%async_computation.1 | async-start | bytes 5242880 | tf_op jit(solution)/shard_map/all_gather | solution.py:303
  12.8 228.4 %all-gather.13.cloned.1.call-start = ((), (), s32[]{:S(2)}) async-start(), calls=%async_computation.2 | async-start | bytes 5242880 | tf_op jit(solution)/shard_map/all_gather | solution.py:303
  13.6 294.4 %all-gather.15.cloned.1.call-start = ((), (), s32[]{:S(2)}) async-start(), calls=%async_computation.3 | async-start | bytes 5242880 | tf_op jit(solution)/shard_map/all_gather | solution.py:303
  81.5 3.2 copy-start.8
  81.5 3.2 copy-start.9
  81.5 3.2 copy-start.10
  81.5 3.2 copy-start.11
  87.6 6.1 %copy-start.5 = (bf16[512,4096]{1,0:T(8,128)(2,1)S(1)}, bf16[512,4096]{1,0:T(8,128)(2,1)}, u32[]{:S(2)}) copy-start(bf16[512,4096]{1,0:T(8,128)(2,1)} %get-tuple-element.9) | copy-start | bytes 12582916
  87.6 6.1 %copy-start.13 = (bf16[4096,512]{1,0:T(8,128)(2,1)S(1)}, bf16[4096,512]{1,0:T(8,128)(2,1)}, u32[]{:S(2)}) copy-start(bf16[4096,512]{1,0:T(8,128)(2,1)} %get-tuple-element.10) | copy-start | bytes 12582916
  93.7 5.6 %copy-start.12 = (f32[2,512]{1,0:T(2,128)S(1)}, f32[2,512]{1,0:T(2,128)}, u32[]{:S(2)}) copy-start(f32[2,512]{1,0:T(2,128)} %param.19) | copy-start | bytes 12292
  96.1 5.4 %collective-permute-start = (bf16[30,512]{1,0:T(8,128)(2,1)S(1)}, bf16[30,512]{1,0:T(8,128)(2,1)S(1)}, u32[]{:S(2)}, u32[]{:S(2)}) collective-permute-start(bf16[30,512]{1,0:T(8,128)(2,1)S(1)} %slice.564), channel_id=1, source_target_pairs={{0,8},{8,16},{16,24},{1,9},{9,17},{17,25},{2,10},{10,18},{18,26},{... | collective-permute-start | bytes 92168 | tf_op jit(solution)/shard_map/ppermute | solution.py:288
  107.4 6.1 %copy-start.4 = (f32[512,512]{1,0:T(8,128)S(1)}, f32[512,512]{1,0:T(8,128)}, u32[]{:S(2)}) copy-start(f32[512,512]{1,0:T(8,128)} %get-tuple-element.18) | copy-start | bytes 3145732
  155.6 1.9 copy-start.2
  241.3 6.2 %copy-start.6 = (bf16[512,4096]{1,0:T(8,128)(2,1)S(1)}, bf16[512,4096]{1,0:T(8,128)(2,1)}, u32[]{:S(2)}) copy-start(bf16[512,4096]{1,0:T(8,128)(2,1)} %get-tuple-element.11) | copy-start | bytes 12582916
  241.3 6.2 %copy-start.14 = (bf16[4096,512]{1,0:T(8,128)(2,1)S(1)}, bf16[4096,512]{1,0:T(8,128)(2,1)}, u32[]{:S(2)}) copy-start(bf16[4096,512]{1,0:T(8,128)(2,1)} %get-tuple-element.12) | copy-start | bytes 12582916
  249.8 5.0 %collective-permute-start.1 = (bf16[30,512]{1,0:T(8,128)(2,1)S(1)}, bf16[30,512]{1,0:T(8,128)(2,1)S(1)}, u32[]{:S(2)}, u32[]{:S(2)}) collective-permute-start(bf16[30,512]{1,0:T(8,128)(2,1)S(1)} %slice.596), channel_id=1, source_target_pairs={{0,8},{8,16},{16,24},{1,9},{9,17},{17,25},{2,10},{10,18},{18,26},{... | collective-permute-start | bytes 92168 | tf_op jit(solution)/shard_map/ppermute | solution.py:288
  306.0 2.0 copy-start.3
Sparse Core Ops, SparseCore 0:
  9.7 77.8 all-gather.8
  89.4 52.7 all-gather.10
  144.1 74.8 all-gather.12
  220.6 52.8 all-gather.14

commit v3 on v2

--- a/solution.py
+++ b/solution.py
@@ -305,7 +305,10 @@
     stream = tokens
     for layer_index in range(layer_count):
         gate_block, out_block = whole[layer_index]
-        gathered, value_block = gather_over_tp(stream, 4 * layer_index, w_value, layer_index)
+        if layer_index == 0:
+            gathered, value_block = gather_over_tp(stream, 0, w_value, 0)
+        else:
+            gathered, value_block = gather_over_tp(stream, 4 * layer_index), next_value
         full_rows = gathered.astype(jnp.float32)
         scale_rows = lax.rsqrt(jnp.mean(full_rows * full_rows, axis=-1, keepdims=True) + 1e-06)
         normed = (full_rows * scale_rows * pre_gain[layer_index]).astype(jnp.bfloat16)
@@ -329,7 +332,12 @@
         mixed = jax.nn.silu(shaped * norm_gain[layer_index] + norm_bias[layer_index]).astype(
             jnp.bfloat16
         )
-        whole_mixed = gather_over_tp(mixed, 4 * layer_index + 2)
+        if layer_index + 1 < layer_count:
+            whole_mixed, next_value = gather_over_tp(
+                mixed, 4 * layer_index + 2, w_value, layer_index + 1
+            )
+        else:
+            whole_mixed = gather_over_tp(mixed, 4 * layer_index + 2)
         branch_low = jnp.dot(whole_mixed, out_block, preferred_element_type=jnp.float32).astype(
             jnp.bfloat16
         )

time: 328 us -> 324 us (0.988)
  transfers between devices with their start and end apart: 6 -> 6, of which waited for: 3 -> 3; matrix products, arithmetic and copies ran while one was open for 14% -> 13% of each run, Pallas kernels for 72% -> 72%
where the time goes in v3:
time: 324 us
  Pallas kernels  238 us (73%)
  matrix products  28.7 us (9%)
  other arithmetic  17.6 us (5%)
  between operations  13.6 us (4%)
  local copies, waits for them, and re-layouts  10.4 us (3%)
  waiting for transfers between devices  8.4 us (3%)
  starting transfers between devices  7.02 us (2%)
    pallas_call x4, Pallas kernels, gather_over_tp(): pl.pallas_call(functools.partial(gather_kernel, chips, ring, layer), out_...  215 us
    pallas_call x4, Pallas kernels, sum_over_tp(): pl.pallas_call(functools.partial(sum_kernel, count), out_shape=jax.ShapeD...  22.9 us
    dot_general x2, matrix products, shards(): gate_proj = jnp.dot(normed, gate_block, preferred_element_type=jnp.float32)  12.2 us
    dot_general x2, matrix products, shards(): jnp.dot(whole_mixed, out_block, preferred_element_type=jnp.float32)  11.6 us
    reduce_sum x2, other arithmetic, shards(): jnp.sum(filtered, axis=-1)  10.7 us
    ppermute x2, starting transfers between devices, passed_along(): lax.ppermute(value, axis, [(source, source + steps) for source in range(l...  6.89 us
  transfers between devices with their start and end apart: 6, of which 3 were waited for; matrix products, arithmetic and copies ran while one was open for 13% of the time, Pallas kernels for 72%

profile of v3, /device:TPU:0, one launch (start us, length us, event | category | flops | bytes accessed | tf_op | source)
XLA Modules:
  0.0 323.7 jit_solution(14642878217838792987)
XLA Ops:
  6.5 3.0 fusion.131
  9.5 0.0 all-gather.9.cloned.1.call-update
  9.6 0.0 all-gather.11.cloned.1.call-start
  9.6 3.2 fusion.130
  12.8 0.0 all-gather.11.cloned.1.call-update
  12.8 0.0 all-gather.13.cloned.1.call-start
  12.9 0.7 all-gather.13.cloned.1.call-update
  13.6 0.0 all-gather.15.cloned.1.call-start
  13.6 0.5 all-gather.15.cloned.1.call-update
  14.3 67.2 %gather_tp.4 = (bf16[512,4096]{1,0:T(8,128)(2,1)}, bf16[4096,512]{1,0:T(8,128)(2,1)}) custom-call(bf16[512,512]{1,0:T(8,128)(2,1)S(1)} %copy-done.2, bf16[2,1024,512]{2,1,0:T(8,128)(2,1)S(1)} %copy-done.3), custom_call_target="tpu_custom_call" | custom-call | flops 20000000000 | bytes 4194304 | tf_op jit(solution)/shard_map/gather_tp/pallas_call | solution.py:209
  81.5 0.0 copy-start.8
  81.5 0.0 copy-start.9
  81.5 0.0 copy-start.10
  81.5 0.0 copy-start.11
  81.5 3.1 fusion
  84.7 2.8 all-gather.9.cloned.1.call-done
  87.6 6.1 %fusion.35 = f32[512,512]{1,0:T(8,128)S(1)} fusion(bf16[1,4096,512]{2,1,0:T(8,128)(2,1)} %all-gather.9.cloned.1.call-done, bf16[512,4096]{1,0:T(8,128)(2,1)} %get-tuple-element.9, f32[4096]{0:T(1024)S(1)} %bitcast.146, f32[512]{0:T(512)S(1)} %add_rsqrt_fusion.1), kind=kOutput, calls=%fused_computation.31 | convolution fusion | flops 2156658688 | bytes 9455616 | tf_op jit(solution)/shard_map/dot_general | solution.py:316
  93.7 2.5 fusion.38
  96.2 3.2 collective-permute-start
  99.5 2.1 collective-permute-done
  101.6 0.2 maximum_convert_fusion
  101.7 5.7 %fusion.127 = (f32[512]{0:T(512)S(1)}, f32[512]{0:T(512)S(1)}, f32[512,512]{1,0:T(8,128)}) fusion(f32[512]{0:T(512)S(1)} %bitcast.178, f32[542,512]{1,0:T(8,128)S(1)} %maximum_convert_fusion, f32[512]{0:T(512)S(1)} %bitcast.179, f32[512]{0:T(512)S(1)} %bitcast.180, f32[512]{0:T(512)S(1)} %bitcast.181, f32[512]{0:T(512)S(1)} %bitcast.182, ...), kind=kLoop, calls=%fused_computation.191 | loop fusion | flops 17038336 | bytes 33624064 | tf_op jit(solution)/shard_map/reduce_sum | solution.py:327
  107.5 6.0 %sum_tp.4 = f32[8,128]{1,0:T(8,128)S(1)} custom-call(f32[8,128]{1,0:T(8,128)S(1)} %reshape.162.x_ref), custom_call_target="tpu_custom_call" | custom-call | flops 2500000000 | bytes 8192 | tf_op jit(solution)/shard_map/sum_tp/pallas_call | solution.py:264
  113.5 0.4 multiply_convert_fusion.1.refs_0_
  114.0 67.1 %gather_tp.5 = (bf16[512,4096]{1,0:T(8,128)(2,1)}, bf16[4096,512]{1,0:T(8,128)(2,1)}) custom-call(bf16[512,512]{1,0:T(8,128)(2,1)S(1)} %multiply_convert_fusion.1.refs_0_, bf16[2,1024,512]{2,1,0:T(8,128)(2,1)S(1)} %copy-done.3), custom_call_target="tpu_custom_call" | custom-call | flops 20000000000 | bytes 4194304 | tf_op jit(solution)/shard_map/gather_tp/pallas_call | solution.py:209
  181.1 0.0 all-gather.11.cloned.1.call-done
  181.1 5.8 %fusion.40 = bf16[512,512]{1,0:T(8,128)(2,1)S(1)} fusion(bf16[512,4096]{1,0:T(8,128)(2,1)} %get-tuple-element.11, bf16[1,4096,512]{2,1,0:T(8,128)(2,1)} %all-gather.11.cloned.1.call-done), kind=kOutput, calls=%fused_computation.34 | convolution fusion | flops 2147745792 | bytes 8912896 | tf_op jit(solution)/shard_map/dot_general | solution.py:341
  186.9 0.2 fusion.50
  187.1 5.6 %sum_tp.5 = f32[4,128]{1,0:T(4,128)S(1)} custom-call(f32[4,128]{1,0:T(4,128)S(1)} %bitcast.142), custom_call_target="tpu_custom_call" | custom-call | flops 2500000000 | bytes 4096 | tf_op jit(solution)/shard_map/sum_tp/pallas_call | solution.py:264
  192.7 0.3 fusion.53.refs_0_
  193.0 40.9 %gather_tp.6 = bf16[512,4096]{1,0:T(8,128)(2,1)S(1)} custom-call(bf16[512,512]{1,0:T(8,128)(2,1)S(1)} %fusion.53.refs_0_), custom_call_target="tpu_custom_call" | custom-call | flops 20000000000 | bytes 4194304 | tf_op jit(solution)/shard_map/gather_tp/pallas_call | solution.py:209
  233.9 2.0 copy-done
  235.9 0.9 fusion.3
  236.8 0.0 all-gather.13.cloned.1.call-done
  236.8 6.1 %fusion.29 = f32[512,512]{1,0:T(8,128)S(1)} fusion(bf16[1,4096,512]{2,1,0:T(8,128)(2,1)} %all-gather.13.cloned.1.call-done, bf16[512,4096]{1,0:T(8,128)(2,1)} %copy-done, f32[4096]{0:T(1024)S(1)} %bitcast.144, f32[512]{0:T(512)S(1)} %add_rsqrt_fusion), kind=kOutput, calls=%fused_computation.29 | convolution fusion | flops 2156658688 | bytes 9455616 | tf_op jit(solution)/shard_map/dot_general | solution.py:316
  243.0 2.4 fusion.39
  245.4 3.7 %collective-permute-start.1 = (bf16[30,512]{1,0:T(8,128)(2,1)S(1)}, bf16[30,512]{1,0:T(8,128)(2,1)S(1)}, u32[]{:S(2)}, u32[]{:S(2)}) collective-permute-start(bf16[30,512]{1,0:T(8,128)(2,1)S(1)} %slice.596), channel_id=1, source_target_pairs={{0,8},{8,16},{16,24},{1,9},{9,17},{17,25},{2,10},{10,18},{18,26},{... | collective-permute-start | bytes 92168 | tf_op jit(solution)/shard_map/ppermute | solution.py:288
  249.1 2.2 collective-permute-done.1
  251.3 0.2 maximum_convert_fusion.1
  251.5 5.0 %fusion.126 = (f32[512]{0:T(512)S(1)}, f32[512]{0:T(512)S(1)}, f32[512,512]{1,0:T(8,128)S(1)}) fusion(f32[512]{0:T(512)S(1)} %bitcast.159, f32[542,512]{1,0:T(8,128)S(1)} %maximum_convert_fusion.1, f32[512]{0:T(512)S(1)} %bitcast.148, f32[512]{0:T(512)S(1)} %bitcast.192, f32[512]{0:T(512)S(1)} %bitcast.193, f32[512]{0:T(512)S(1)} %bitcast.194, ...), kind=kLoop, calls=%fused_computation.190 | loop fusion | flops 17038336 | bytes 33624064 | tf_op jit(solution)/shard_map/reduce_sum | solution.py:327
  256.5 5.6 %sum_tp.6 = f32[8,128]{1,0:T(8,128)S(1)} custom-call(f32[8,128]{1,0:T(8,128)S(1)} %reshape.163.x_ref), custom_call_target="tpu_custom_call" | custom-call | flops 2500000000 | bytes 8192 | tf_op jit(solution)/shard_map/sum_tp/pallas_call | solution.py:264
  262.2 0.4 multiply_convert_fusion.refs_0_
  262.6 39.9 %gather_tp.7 = bf16[512,4096]{1,0:T(8,128)(2,1)S(1)} custom-call(bf16[512,512]{1,0:T(8,128)(2,1)S(1)} %multiply_convert_fusion.refs_0_), custom_call_target="tpu_custom_call" | custom-call | flops 20000000000 | bytes 4194304 | tf_op jit(solution)/shard_map/gather_tp/pallas_call | solution.py:209
  302.5 2.0 copy-done.4
  304.5 5.8 %fusion.43 = bf16[512,512]{1,0:T(8,128)(2,1)S(1)} fusion(bf16[512,4096]{1,0:T(8,128)(2,1)} %copy-done.4, bf16[1,4096,512]{2,1,0:T(8,128)(2,1)} %all-gather.15.cloned.1.call-done), kind=kOutput, calls=%fused_computation.35 | convolution fusion | flops 2147745792 | bytes 8912896 | tf_op jit(solution)/shard_map/dot_general | solution.py:341
  310.3 0.2 fusion.54
  310.4 5.6 %sum_tp.7 = f32[4,128]{1,0:T(4,128)S(1)} custom-call(f32[4,128]{1,0:T(4,128)S(1)} %bitcast.143), custom_call_target="tpu_custom_call" | custom-call | flops 2500000000 | bytes 4096 | tf_op jit(solution)/shard_map/sum_tp/pallas_call | solution.py:264
  316.1 1.1 fusion.57
  (49 shorter events, 0.4 us)
Async XLA Ops:
  6.5 81.0 %all-gather.9.cloned.1.call-start = ((), (), s32[]{:S(2)}) async-start(), calls=%async_computation | async-start | bytes 5242880 | tf_op jit(solution)/shard_map/all_gather | solution.py:303
  9.5 4.6 %copy-start.7 = (f32[2,31,512]{2,0,1:T(2,128)S(1)}, f32[2,31,512]{2,0,1:T(2,128)}, u32[]{:S(2)}) copy-start(f32[2,31,512]{2,0,1:T(2,128)} %param.14) | copy-start | bytes 380932
  9.5 4.7 %copy-start.2 = (bf16[512,512]{1,0:T(8,128)(2,1)S(1)}, bf16[512,512]{1,0:T(8,128)(2,1)}, u32[]{:S(2)}) copy-start(bf16[512,512]{1,0:T(8,128)(2,1)} %refs_0_.1) | copy-start | bytes 1572868
  9.5 4.7 %copy-start.3 = (bf16[2,1024,512]{2,1,0:T(8,128)(2,1)S(1)}, bf16[2,1024,512]{2,1,0:T(8,128)(2,1)}, u32[]{:S(2)}) copy-start(bf16[2,1024,512]{2,1,0:T(8,128)(2,1)} %refs_1_.3) | copy-start | bytes 6291460
  9.6 171.5 %all-gather.11.cloned.1.call-start = ((), (), s32[]{:S(2)}) async-start(), calls=%async_computation.1 | async-start | bytes 5242880 | tf_op jit(solution)/shard_map/all_gather | solution.py:303
  12.8 224.0 %all-gather.13.cloned.1.call-start = ((), (), s32[]{:S(2)}) async-start(), calls=%async_computation.2 | async-start | bytes 5242880 | tf_op jit(solution)/shard_map/all_gather | solution.py:303
  13.6 290.9 %all-gather.15.cloned.1.call-start = ((), (), s32[]{:S(2)}) async-start(), calls=%async_computation.3 | async-start | bytes 5242880 | tf_op jit(solution)/shard_map/all_gather | solution.py:303
  81.5 3.2 copy-start.8
  81.5 3.2 copy-start.9
  81.5 3.2 copy-start.10
  81.5 3.2 copy-start.11
  87.6 6.1 %copy-start.6 = (bf16[512,4096]{1,0:T(8,128)(2,1)S(1)}, bf16[512,4096]{1,0:T(8,128)(2,1)}, u32[]{:S(2)}) copy-start(bf16[512,4096]{1,0:T(8,128)(2,1)} %get-tuple-element.9) | copy-start | bytes 12582916
  87.6 6.1 %copy-start.14 = (bf16[4096,512]{1,0:T(8,128)(2,1)S(1)}, bf16[4096,512]{1,0:T(8,128)(2,1)}, u32[]{:S(2)}) copy-start(bf16[4096,512]{1,0:T(8,128)(2,1)} %get-tuple-element.10) | copy-start | bytes 12582916
  93.7 5.7 %copy-start.12 = (f32[2,512]{1,0:T(2,128)S(1)}, f32[2,512]{1,0:T(2,128)}, u32[]{:S(2)}) copy-start(f32[2,512]{1,0:T(2,128)} %param.19) | copy-start | bytes 12292
  96.2 5.4 %collective-permute-start = (bf16[30,512]{1,0:T(8,128)(2,1)S(1)}, bf16[30,512]{1,0:T(8,128)(2,1)S(1)}, u32[]{:S(2)}, u32[]{:S(2)}) collective-permute-start(bf16[30,512]{1,0:T(8,128)(2,1)S(1)} %slice.564), channel_id=1, source_target_pairs={{0,8},{8,16},{16,24},{1,9},{9,17},{17,25},{2,10},{10,18},{18,26},{... | collective-permute-start | bytes 92168 | tf_op jit(solution)/shard_map/ppermute | solution.py:288
  107.5 6.0 %copy-start.5 = (f32[512,512]{1,0:T(8,128)S(1)}, f32[512,512]{1,0:T(8,128)}, u32[]{:S(2)}) copy-start(f32[512,512]{1,0:T(8,128)} %get-tuple-element.18) | copy-start | bytes 3145732
  233.9 2.0 copy-start
  236.8 6.1 %copy-start.1 = (bf16[512,4096]{1,0:T(8,128)(2,1)S(1)}, bf16[512,4096]{1,0:T(8,128)(2,1)}, u32[]{:S(2)}) copy-start(bf16[512,4096]{1,0:T(8,128)(2,1)} %copy-done) | copy-start | bytes 12582916
  236.8 6.1 %copy-start.13 = (bf16[4096,512]{1,0:T(8,128)(2,1)S(1)}, bf16[4096,512]{1,0:T(8,128)(2,1)}, u32[]{:S(2)}) copy-start(bf16[4096,512]{1,0:T(8,128)(2,1)} %get-tuple-element.12) | copy-start | bytes 12582916
  245.4 5.9 %collective-permute-start.1 = (bf16[30,512]{1,0:T(8,128)(2,1)S(1)}, bf16[30,512]{1,0:T(8,128)(2,1)S(1)}, u32[]{:S(2)}, u32[]{:S(2)}) collective-permute-start(bf16[30,512]{1,0:T(8,128)(2,1)S(1)} %slice.596), channel_id=1, source_target_pairs={{0,8},{8,16},{16,24},{1,9},{9,17},{17,25},{2,10},{10,18},{18,26},{... | collective-permute-start | bytes 92168 | tf_op jit(solution)/shard_map/ppermute | solution.py:288
  302.5 2.0 copy-start.4
Sparse Core Ops, SparseCore 0:
  9.7 77.8 all-gather.8
  89.4 75.0 all-gather.10
  166.4 52.7 all-gather.12
  220.9 52.8 all-gather.14
